TPU v7x, 32 devices: a whole 2x2x4 slice. The times are simulated.
32 devices in a mesh: sp: 8 (over z, y), tp: 4 (over x, core).
Axes of the slice: x: 2, y: 2, z: 4, core: 2. Of those that a mesh axis runs over, the one named last changes fastest.
Arguments:
- hidden: bfloat16 [6144, 2048], P(('sp', 'tp')), may hold values from -6 to 6
- norm_gain: float32 [2, 2048], replicated, may hold values from 0.1 to 1.9
- w_value: bfloat16 [2, 2048, 2048], P(None, 'sp', 'tp'), may hold values from -0.125 to 0.125
- w_gate: bfloat16 [2, 2048, 2048], P(None, 'sp', 'tp'), may hold values from -0.125 to 0.125
- conv_weight: float32 [2, 31, 2048], P(None, None, 'tp'), may hold values from -3 to 3
- conv_bias: float32 [2, 2048], P(None, 'tp'), may hold values from -3 to 3
- chan_gain: float32 [2, 2048], P(None, 'tp'), may hold values from 0.1 to 1.9
- chan_shift: float32 [2, 2048], P(None, 'tp'), may hold values from -3 to 3
- w_out: bfloat16 [2, 2048, 2048], P(None, 'tp', 'sp'), may hold values from -0.125 to 0.125
Outputs:
- result: bfloat16 [6144, 2048], P(('sp', 'tp'))
All inputs are finite; a program needn't handle non-finite values.
Results may differ from a plain program's by a relative error of at most 0.015.
Values may be sent and summed in bfloat16 or wider, within the bound.
A program may use at most 64 MiB of HBM per device.

v0:
```python
import jax
import jax.numpy as jnp
from jax import lax
from jax.sharding import PartitionSpec as P

EPS = 1e-06


def shifted(shard, axis, by):
    size = lax.axis_size(axis)
    pairs = [(i, i + by) for i in range(size) if 0 <= i + by < size]
    return lax.ppermute(shard, axis, pairs)


def body(hidden, norm_gain, w_value, w_gate, conv_weight, conv_bias, chan_gain, chan_shift, w_out):
    group = lax.axis_size("tp")
    own_rows = hidden.shape[0]
    chans = w_value.shape[2]
    taps = conv_weight.shape[1]
    state = hidden
    for layer in range(norm_gain.shape[0]):
        xf = state.astype(jnp.float32)
        scale = lax.rsqrt(jnp.mean(xf * xf, axis=1, keepdims=True) + EPS)
        normed = (xf * scale * norm_gain[layer][None, :]).astype(jnp.bfloat16)
        tokens = lax.all_gather(normed, "tp", axis=0, tiled=True)
        empty = jnp.zeros((tokens.shape[0], chans), jnp.float32)

        def add_both(totals, pieces, start, tokens=tokens):
            return (
                jnp.dot(tokens, pieces[0], preferred_element_type=jnp.float32),
                jnp.dot(tokens, pieces[1], preferred_element_type=jnp.float32),
            )

        lin, gate = add_both(
            (empty, empty),
            (
                lax.all_gather(w_value[layer], "sp", axis=0, tiled=True),
                lax.all_gather(w_gate[layer], "sp", axis=0, tiled=True),
            ),
            jnp.int32(0),
        )
        glu = (lin * jax.nn.sigmoid(gate)).astype(jnp.bfloat16)
        before = shifted(glu[tokens.shape[0] - (taps - 1) :], "sp", 1)
        window = jnp.concatenate([before, glu], axis=0).astype(jnp.float32)
        length = tokens.shape[0]
        mixed = jnp.zeros((length, chans), jnp.float32) + conv_bias[layer][None, :]
        for tap in range(taps):
            mixed = mixed + conv_weight[layer, tap][None, :] * window[tap : tap + length]
        totals = lax.psum((jnp.sum(mixed, axis=1), jnp.sum(mixed * mixed, axis=1)), "tp")
        mean = (totals[0] / (chans * group))[:, None]
        msq = (totals[1] / (chans * group))[:, None]
        var = msq - mean * mean
        act = jax.nn.silu(
            (mixed - mean) * lax.rsqrt(var + EPS) * chan_gain[layer][None, :]
            + chan_shift[layer][None, :]
        ).astype(jnp.bfloat16)

        def project(piece, start, act=act):
            return jnp.dot(act, piece, preferred_element_type=jnp.float32)

        partial_out = project(lax.all_gather(w_out[layer], "sp", axis=1, tiled=True), jnp.int32(0))

        def take_rows(start, count, partial_out=partial_out):
            return partial_out

        update = lax.psum_scatter(
            take_rows(jnp.int32(0), own_rows * lax.axis_size("tp")).astype(jnp.bfloat16),
            "tp",
            scatter_dimension=0,
            tiled=True,
        ).astype(jnp.float32)
        state = (xf + update).astype(jnp.bfloat16)
    return state


def solution(mesh):
    placed = (
        P(("sp", "tp"), None),
        P(),
        P(None, "sp", "tp"),
        P(None, "sp", "tp"),
        P(None, None, "tp"),
        P(None, "tp"),
        P(None, "tp"),
        P(None, "tp"),
        P(None, "tp", "sp"),
    )
    return jax.shard_map(
        body, mesh=mesh, in_specs=placed, out_specs=P(("sp", "tp"), None), check_vma=False
    )
```

profile of v0, /device:TPU:0, one launch (start us, length us, event | category | flops | bytes accessed | tf_op | source)
XLA Modules:
  0.0 466.3 jit_solution(699687578448124518)
XLA Ops:
  6.5 0.0 all-gather.21.cloned.1.call-start
  6.5 2.0 fusion.101
  8.5 0.0 all-gather.21.cloned.1.call-update
  8.5 0.0 copy-start.2
  8.5 0.0 all-gather.15.cloned.1.call-start
  8.6 0.0 copy-done
  8.6 0.2 fusion.10
  8.9 0.0 copy-done.5
  8.9 0.0 copy-start.3
  8.9 1.1 fusion.12
  10.0 0.0 all-gather.15.cloned.1.call-update
  10.0 0.0 copy-start.6
  10.1 0.0 copy-start.7
  10.1 0.0 all-gather.19.cloned.1.call-start
  10.1 0.0 copy-done.2
  10.1 0.8 fusion.100
  11.0 0.0 all-gather.19.cloned.1.call-update
  11.0 0.0 all-gather.23.cloned.1.call-start
  11.0 0.0 copy-done.3
  11.1 0.8 fusion.102
  11.9 0.0 all-gather.23.cloned.1.call-update
  11.9 0.0 reduce-scatter.3.cloned.1.call-start
  12.1 49.2 %all-gather.21.cloned.1.call-done = bf16[1,2048,512]{2,1,0:T(8,128)(2,1)} async-done(((bf16[1,256,512]{2,1,0:T(8,128)(2,1)}), bf16[1,2048,512]{2,1,0:T(8,128)(2,1)}) %all-gather.21.cloned.1.call-update) | async-done | bytes 2097168 | tf_op jit(solution)/shard_map/all_gather | solution.py:38
  61.3 28.6 %all-gather.15.cloned.1.call-done = bf16[768,2048]{1,0:T(8,128)(2,1)} async-done(((bf16[192,2048]{1,0:T(8,128)(2,1)}), bf16[768,2048]{1,0:T(8,128)(2,1)}) %all-gather.15.cloned.1.call-update) | async-done | bytes 3145744 | tf_op jit(solution)/shard_map/all_gather | solution.py:25
  89.9 4.3 fusion.6
  94.3 0.0 copy-start.8
  94.3 46.9 %all-gather.19.cloned.1.call-done = bf16[1,2048,512]{2,1,0:T(8,128)(2,1)} async-done(((bf16[1,256,512]{2,1,0:T(8,128)(2,1)}), bf16[1,2048,512]{2,1,0:T(8,128)(2,1)}) %all-gather.19.cloned.1.call-update) | async-done | bytes 2097168 | tf_op jit(solution)/shard_map/all_gather | solution.py:37
  141.2 4.5 multiply_convert_fusion.3
  145.7 2.5 collective-permute-start
  148.2 0.0 copy-done.8
  148.2 1.6 collective-permute-done
  149.7 0.2 maximum_convert_fusion
  150.0 6.9 %fusion.97 = (f32[768]{0:T(1024)S(1)}, f32[768]{0:T(1024)S(1)}, f32[768,512]{1,0:T(8,128)S(1)}) fusion(f32[798,512]{1,0:T(8,128)S(1)} %maximum_convert_fusion, f32[512]{0:T(512)S(1)} %bitcast.128, f32[512]{0:T(512)S(1)} %bitcast.129, f32[512]{0:T(512)S(1)} %bitcast.130, f32[512]{0:T(512)S(1)} %bitcast.131, f32[512]{0:T(512)S(1)} %bitcast.132, ...), kind=kLoop, calls=%fused_computation.177 | loop fusion | flops 25557504 | bytes 50403328 | tf_op jit(solution)/shard_map/reduce_sum | solution.py:49
  156.9 6.2 %all-reduce.1 = (f32[768]{0:T(1024)S(1)}, f32[768]{0:T(1024)S(1)}) all-reduce(f32[768]{0:T(1024)S(1)} %get-tuple-element.8, f32[768]{0:T(1024)S(1)} %get-tuple-element.7), channel_id=1, replica_groups=mesh['sp'=8,'tp'=4] {'tp'}, use_global_device_ids=true, to_apply=%region_4.0 | all-reduce | flops 1536 | bytes 12288 | tf_op jit(solution)/shard_map/psum | solution.py:49
  163.1 28.9 %all-gather.23.cloned.1.call-done = bf16[1,512,2048]{2,1,0:T(8,128)(2,1)} async-done(((bf16[1,512,256]{2,1,0:T(8,128)(2,1)}), bf16[1,512,2048]{2,1,0:T(8,128)(2,1)}) %all-gather.23.cloned.1.call-update) | async-done | bytes 2097168 | tf_op jit(solution)/shard_map/all_gather | solution.py:61
  192.0 5.3 %convolution_convert_fusion.1 = bf16[768,2048]{1,0:T(8,128)(2,1)} fusion(bf16[1,512,2048]{2,1,0:T(8,128)(2,1)} %all-gather.23.cloned.1.call-done, f32[768,512]{1,0:T(8,128)S(1)} %get-tuple-element.14, f32[512]{0:T(512)S(1)} %bitcast.165, f32[512]{0:T(512)S(1)} %bitcast.164, f32[768]{0:T(1024)S(1)} %get-tuple-element.94, f32[768]{0:T(1024)S(1)} %get-tuple-element.93), kind=kOutput, calls=%fused_computation.1 | convolution fusion | flops 1615724544 | bytes 6825984 | tf_op jit(solution)/shard_map/dot_general | solution.py:59
  197.3 0.0 reduce-scatter.3.cloned.1.call-update
  197.4 0.0 all-gather.27.cloned.1.call-start
  197.4 0.5 all-gather.27.cloned.1.call-update
  197.9 0.0 all-gather.17.cloned.1.call-start
  198.0 35.6 %reduce-scatter.3.cloned.1.call-done = bf16[192,2048]{1,0:T(8,128)(2,1)} async-done(((bf16[768,2048]{1,0:T(8,128)(2,1)}), bf16[192,2048]{1,0:T(8,128)(2,1)}) %reduce-scatter.3.cloned.1.call-update) | async-done | bytes 786448 | tf_op jit(solution)/shard_map/reduce_scatter | solution.py:66
  233.5 1.5 fusion.14
  235.1 1.2 fusion.16
  236.3 0.0 all-gather.17.cloned.1.call-update
  236.4 0.0 all-gather.25.cloned.1.call-start
  236.4 0.7 all-gather.25.cloned.1.call-update
  237.1 0.0 all-gather.29.cloned.1.call-start
  237.2 0.7 all-gather.29.cloned.1.call-update
  237.8 0.0 reduce-scatter.5.cloned.1.call-start
  237.9 46.8 %all-gather.27.cloned.1.call-done = bf16[1,2048,512]{2,1,0:T(8,128)(2,1)} async-done(((bf16[1,256,512]{2,1,0:T(8,128)(2,1)}), bf16[1,2048,512]{2,1,0:T(8,128)(2,1)}) %all-gather.27.cloned.1.call-update) | async-done | bytes 2097168 | tf_op jit(solution)/shard_map/all_gather | solution.py:38
  284.7 28.6 %all-gather.17.cloned.1.call-done = bf16[768,2048]{1,0:T(8,128)(2,1)} async-done(((bf16[192,2048]{1,0:T(8,128)(2,1)}), bf16[768,2048]{1,0:T(8,128)(2,1)}) %all-gather.17.cloned.1.call-update) | async-done | bytes 3145744 | tf_op jit(solution)/shard_map/all_gather | solution.py:25
  313.3 4.3 fusion.1
  317.6 46.9 %all-gather.25.cloned.1.call-done = bf16[1,2048,512]{2,1,0:T(8,128)(2,1)} async-done(((bf16[1,256,512]{2,1,0:T(8,128)(2,1)}), bf16[1,2048,512]{2,1,0:T(8,128)(2,1)}) %all-gather.25.cloned.1.call-update) | async-done | bytes 2097168 | tf_op jit(solution)/shard_map/all_gather | solution.py:37
  364.5 4.5 multiply_convert_fusion.1
  369.0 2.7 collective-permute-start.1
  371.7 1.3 collective-permute-done.1
  373.1 0.2 maximum_convert_fusion.1
  373.3 6.9 %fusion.96 = (f32[768]{0:T(1024)S(1)}, f32[768]{0:T(1024)S(1)}, f32[768,512]{1,0:T(8,128)S(1)}) fusion(f32[798,512]{1,0:T(8,128)S(1)} %maximum_convert_fusion.1, f32[512]{0:T(512)S(1)} %bitcast.109, f32[512]{0:T(512)S(1)} %bitcast.98, f32[512]{0:T(512)S(1)} %bitcast.142, f32[512]{0:T(512)S(1)} %bitcast.143, f32[512]{0:T(512)S(1)} %bitcast.144, ...), kind=kLoop, calls=%fused_computation.176 | loop fusion | flops 25557504 | bytes 50403328 | tf_op jit(solution)/shard_map/reduce_sum | solution.py:49
  380.2 6.2 %all-reduce = (f32[768]{0:T(1024)S(1)}, f32[768]{0:T(1024)S(1)}) all-reduce(f32[768]{0:T(1024)S(1)} %get-tuple-element.6, f32[768]{0:T(1024)S(1)} %get-tuple-element.5), channel_id=1, replica_groups=mesh['sp'=8,'tp'=4] {'tp'}, use_global_device_ids=true, to_apply=%region_10.11 | all-reduce | flops 1536 | bytes 12288 | tf_op jit(solution)/shard_map/psum | solution.py:49
  386.4 29.1 %all-gather.29.cloned.1.call-done = bf16[1,512,2048]{2,1,0:T(8,128)(2,1)} async-done(((bf16[1,512,256]{2,1,0:T(8,128)(2,1)}), bf16[1,512,2048]{2,1,0:T(8,128)(2,1)}) %all-gather.29.cloned.1.call-update) | async-done | bytes 2097168 | tf_op jit(solution)/shard_map/all_gather | solution.py:61
  415.5 5.3 %convolution_convert_fusion = bf16[768,2048]{1,0:T(8,128)(2,1)} fusion(bf16[1,512,2048]{2,1,0:T(8,128)(2,1)} %all-gather.29.cloned.1.call-done, f32[768,512]{1,0:T(8,128)S(1)} %get-tuple-element.13, f32[512]{0:T(512)S(1)} %bitcast.163, f32[512]{0:T(512)S(1)} %bitcast.162, f32[768]{0:T(1024)S(1)} %get-tuple-element.86, f32[768]{0:T(1024)S(1)} %get-tuple-element.85), kind=kOutput, calls=%fused_computation | convolution fusion | flops 1615724544 | bytes 6825984 | tf_op jit(solution)/shard_map/dot_general | solution.py:59
  420.8 0.0 reduce-scatter.5.cloned.1.call-update
  420.9 36.2 %reduce-scatter.5.cloned.1.call-done = bf16[192,2048]{1,0:T(8,128)(2,1)} async-done(((bf16[768,2048]{1,0:T(8,128)(2,1)}), bf16[192,2048]{1,0:T(8,128)(2,1)}) %reduce-scatter.5.cloned.1.call-update) | async-done | bytes 786448 | tf_op jit(solution)/shard_map/reduce_scatter | solution.py:66
  457.1 2.4 fusion.17
  (22 shorter events, 0.2 us)
Async XLA Ops:
  6.5 2.1 copy-start
  6.5 2.3 copy-start.5
  6.5 54.8 %all-gather.21.cloned.1.call-start = ((), (), s32[]{:S(2)}) async-start(), calls=%async_computation.7 | async-start | bytes 2359296 | tf_op jit(solution)/shard_map/all_gather | solution.py:38
  8.5 1.6 copy-start.2
  8.5 81.4 %all-gather.15.cloned.1.call-start = ((), (), s32[]{:S(2)}) async-start(), calls=%async_computation.2 | async-start | bytes 3932160 | tf_op jit(solution)/shard_map/all_gather | solution.py:25
  8.9 2.2 copy-start.3
  10.0 2.0 copy-start.4
  10.0 2.0 copy-start.6
  10.1 2.1 copy-start.7
  10.1 131.1 %all-gather.19.cloned.1.call-start = ((), (), s32[]{:S(2)}) async-start(), calls=%async_computation.6 | async-start | bytes 2359296 | tf_op jit(solution)/shard_map/all_gather | solution.py:37
  11.0 181.0 %all-gather.23.cloned.1.call-start = ((), (), s32[]{:S(2)}) async-start(), calls=%async_computation.8 | async-start | bytes 2359296 | tf_op jit(solution)/shard_map/all_gather | solution.py:61
  11.9 221.6 %reduce-scatter.3.cloned.1.call-start = ((), (), s32[]{:S(2)}) async-start(), calls=%async_computation.3 | async-start | bytes 3932160 | tf_op jit(solution)/shard_map/reduce_scatter | solution.py:66
  94.3 53.9 %copy-start.8 = (f32[2,512]{1,0:T(2,128)S(1)}, f32[2,512]{1,0:T(2,128)}, u32[]{:S(2)}) copy-start(f32[2,512]{1,0:T(2,128)} %param.16) | copy-start | bytes 12292
  145.7 4.0 collective-permute-start
  197.4 87.3 %all-gather.27.cloned.1.call-start = ((), (), s32[]{:S(2)}) async-start(), calls=%async_computation.10 | async-start | bytes 2359296 | tf_op jit(solution)/shard_map/all_gather | solution.py:38
  197.9 115.4 %all-gather.17.cloned.1.call-start = ((), (), s32[]{:S(2)}) async-start(), calls=%async_computation.4 | async-start | bytes 3932160 | tf_op jit(solution)/shard_map/all_gather | solution.py:25
  233.5 1.6 copy-start.1
  236.4 128.2 %all-gather.25.cloned.1.call-start = ((), (), s32[]{:S(2)}) async-start(), calls=%async_computation.9 | async-start | bytes 2359296 | tf_op jit(solution)/shard_map/all_gather | solution.py:37
  237.1 178.4 %all-gather.29.cloned.1.call-start = ((), (), s32[]{:S(2)}) async-start(), calls=%async_computation.11 | async-start | bytes 2359296 | tf_op jit(solution)/shard_map/all_gather | solution.py:61
  237.8 219.2 %reduce-scatter.5.cloned.1.call-start = ((), (), s32[]{:S(2)}) async-start(), calls=%async_computation.5 | async-start | bytes 3932160 | tf_op jit(solution)/shard_map/reduce_scatter | solution.py:66
  369.0 4.1 collective-permute-start.1
Sparse Core Ops, SparseCore 0:
  9.5 51.7 all-gather.20
  62.9 27.0 all-gather.14
  92.1 49.0 all-gather.18
  143.1 48.8 all-gather.22
  197.5 36.0 reduce-scatter.2
  235.5 49.0 all-gather.26
  286.2 27.0 all-gather.16
  315.4 49.0 all-gather.24
  366.6 48.8 all-gather.28
  421.0 36.0 reduce-scatter.4
where the time goes:
time: 467 us; the launch traced here: 466 us
  waiting for transfers between devices  382 us (82%)
  matrix products  28.3 us (6%)
  other arithmetic  20.8 us (4%)
  between operations  13.8 us (3%)
  blocking collectives  12.3 us (3%)
  starting transfers between devices  5.48 us (1%)
    all_gather x2, waiting for transfers between devices, body(): lax.all_gather(w_gate[layer], 'sp', axis=0, tiled=True)  95.9 us
    all_gather x2, waiting for transfers between devices, body(): lax.all_gather(w_value[layer], 'sp', axis=0, tiled=True)  93.8 us
    reduce_scatter x2, waiting for transfers between devices, body(): lax.psum_scatter(take_rows(jnp.int32(0), own_rows * lax.axis_size('tp'))....  71.8 us
    all_gather x2, waiting for transfers between devices, body(): lax.all_gather(w_out[layer], 'sp', axis=1, tiled=True)  58 us
    all_gather x2, waiting for transfers between devices, body(): tokens = lax.all_gather(normed, 'tp', axis=0, tiled=True)  57.3 us
    reduce_sum x2, other arithmetic, body(): jnp.sum(mixed, axis=1)  13.8 us
    psum x2, blocking collectives, body(): lax.psum((jnp.sum(mixed, axis=1), jnp.sum(mixed * mixed, axis=1)), 'tp')  12.3 us
    dot_general x2, matrix products, project(): return jnp.dot(act, piece, preferred_element_type=jnp.float32)  10.7 us
  transfers between devices with their start and end apart: 12, of which 12 were waited for; matrix products, arithmetic and copies ran while one was open for 8% of the time, Pallas kernels for 0%

commit v1 on v0

v1 whole, which is shorter than its diff:
```python
import functools

import jax
import jax.numpy as jnp
from jax import lax
from jax.experimental import pallas as pl
from jax.experimental.pallas import tpu as pltpu
from jax.sharding import PartitionSpec as P

EPS = 1e-06
F32 = jnp.float32
BF16 = jnp.bfloat16
MESH = pl.DeviceIdType.MESH
RT = 128
HALO = 32
LANES = 128


def dot(a, b):
    return jnp.dot(a, b, preferred_element_type=F32)


def kernel(Z, Y, X, h_ref, gain_ref, wv_ref, wg_ref, cw_ref, cb_ref, cg_ref, cs_ref, wo_ref, o_ref,
           WV, WG, WO, TOK, PT, PI, PX, RX, GLF, HB, MIX, S1, S2, ST, ACT, HS,
           w_rs, wz_ss, wz2_ss, wy_ss, t_ss, t_rs, h_ss, h_rs, s_ss, s_rs, d_ss, d_rs, x_ss, x_rs):
    L = gain_ref.shape[0]
    own_rows, D = h_ref.shape
    rows = wv_ref.shape[1]
    C = wv_ref.shape[2]
    NT = 2 * X
    M = own_rows * NT
    taps = cw_ref.shape[1]
    wcols = wo_ref.shape[2]
    s = lax.axis_index("sp")
    t = lax.axis_index("tp")
    z, y = s // Y, lax.rem(s, Y)
    x, c = t // 2, lax.rem(t, 2)
    units = [(l, k) for l in range(L) for k in range(3)]
    U = len(units)
    scheme_a = [u == 2 for u in range(U)]

    def wrap(v, n):
        return lax.rem(v + n, n)

    def sdev(zz, yy):
        return (zz * Y + yy, t)

    def tdev(xx, cc):
        return (s, xx * 2 + cc)

    partner = tdev(x, 1 - c)
    nxt = (wrap(s + 1, Z * Y), t)
    prev = (wrap(s - 1, Z * Y), t)
    zp = sdev(wrap(z + 1, Z), y)
    zm = sdev(wrap(z - 1, Z), y)
    has_p, has_m = z + 1 < Z, z >= 1

    bar = pltpu.get_barrier_semaphore()

    def greet(dev):
        pl.semaphore_signal(bar, inc=1, device_id=dev, device_id_type=MESH)

    count = 0
    for yo in range(1, Y):
        greet(sdev(z, wrap(y + yo, Y)))
        count += 1
    for o in range(1, NT):
        greet((s, wrap(t + o, NT)))
        count += 1

    @pl.when(has_p)
    def _():
        greet(zp)

    @pl.when(has_m)
    def _():
        greet(zm)

    @pl.when(s + 1 < Z * Y)
    def _():
        greet(nxt)

    @pl.when(s >= 1)
    def _():
        greet(prev)

    peers = count + sum(cond.astype(jnp.int32) for cond in (has_p, has_m, s + 1 < Z * Y, s >= 1))
    pl.semaphore_wait(bar, peers)

    def piece(u, src):
        l, k = units[u]
        if k == 2:
            return WO.at[l, src]
        w = WV if k == 0 else WG
        return w.at[l, pl.ds(pl.multiple_of(src * rows, rows), rows), :]

    def own_piece(u):
        l, k = units[u]
        return (wv_ref, wg_ref, wo_ref)[k].at[l]

    def wcopy(u, src, dev, ssem, first):
        return pltpu.make_async_remote_copy(
            src_ref=own_piece(u) if first else piece(u, src), dst_ref=piece(u, src),
            send_sem=ssem, recv_sem=w_rs.at[u, src], device_id=dev, device_id_type=MESH)

    pending = []

    def go(cond, make):
        def _():
            make().start()
        if cond is None:
            _()
        else:
            pl.when(cond)(_)
        pending.append((cond, make))

    def drain():
        for cond, make in pending:
            def _(make=make):
                make().wait_send()
            if cond is None:
                _()
            else:
                pl.when(cond)(_)
        pending.clear()

    def wait_w(u, src):
        wcopy(u, src, zp, wz_ss.at[u, src], False).wait_recv()

    def send_own(u):
        go(has_p, lambda: wcopy(u, s, zp, wz_ss.at[u, s], True))
        go(has_m, lambda: wcopy(u, s, zm, wz2_ss.at[u, y], True))
        for yo in range(1, Y):
            go(None, lambda yo=yo: wcopy(u, s, sdev(z, wrap(y + yo, Y)), wy_ss.at[u, z, yo - 1], True))
        l, k = units[u]
        if k == 2:
            WO[l, s] = wo_ref[l]
        else:
            w, r = ((WV, wv_ref), (WG, wg_ref))[k]
            w[l, pl.ds(pl.multiple_of(s * rows, rows), rows), :] = r[l]

    def ev_p(u):
        for yo in range(1, Y):
            yy = wrap(y + yo, Y)
            src = z * Y + yy
            wait_w(u, src)
            go(has_p, lambda src=src: wcopy(u, src, zp, wz_ss.at[u, src], False))
            go(has_m, lambda src=src, yy=yy: wcopy(u, src, zm, wz2_ss.at[u, yy], False))

    def ev_d(u, k):
        for sgn in (1, -1):
            zs = wrap(z - sgn * k, Z)
            valid = z >= k if sgn == 1 else z + k < Z
            fwd = jnp.logical_and(valid, has_p if sgn == 1 else has_m)
            dev = zp if sgn == 1 else zm
            src = zs * Y + y

            @pl.when(valid)
            def _():
                wait_w(u, src)
            go(fwd, lambda src=src, dev=dev: wcopy(u, src, dev, wz_ss.at[u, src], False))
            for yo in range(1, Y):
                yy = wrap(y + yo, Y)
                if scheme_a[u]:
                    src2 = zs * Y + yy

                    @pl.when(valid)
                    def _():
                        wait_w(u, src2)
                    go(fwd, lambda src2=src2, dev=dev: wcopy(u, src2, dev, wz_ss.at[u, src2], False))
                else:
                    go(valid, lambda src=src, yy=yy, yo=yo, zs=zs: wcopy(
                        u, src, sdev(z, yy), wy_ss.at[u, zs, yo - 1], False))

    def zorder(j):
        return jnp.where(z < Z // 2, wrap(z + j, Z), wrap(z - j, Z))

    def fin(u):
        if not scheme_a[u]:
            for j in range(Z):
                for yo in range(1, Y):
                    wait_w(u, zorder(j) * Y + wrap(y + yo, Y))

    def tcopy(l, slot, dev, i):
        ref = TOK.at[l, pl.ds(pl.multiple_of(slot * own_rows, own_rows), own_rows), :]
        return pltpu.make_async_remote_copy(
            src_ref=ref, dst_ref=ref, send_sem=t_ss.at[l, i], recv_sem=t_rs.at[l, slot],
            device_id=dev, device_id_type=MESH)

    NR = own_rows // 4 if own_rows % 64 == 0 else own_rows // 2

    def norm_send(l):
        def nb(i, _):
            r = pl.ds(pl.multiple_of(i * NR, NR), NR)
            xf = (h_ref if l == 0 else HS)[r, :].astype(F32)
            scale = lax.rsqrt(jnp.mean(xf * xf, axis=1, keepdims=True) + EPS)
            TOK[l, pl.ds(pl.multiple_of(t * own_rows + i * NR, NR), NR), :] = (
                xf * scale * gain_ref[l, :][None, :]).astype(BF16)
            return 0
        lax.fori_loop(0, own_rows // NR, nb, 0)
        for o in range(1, X):
            go(None, lambda o=o: tcopy(l, t, tdev(wrap(x + o, X), c), o - 1))
        go(None, lambda: tcopy(l, t, partner, X - 1))

    def tok_relay(l):
        for o in range(1, X):
            slot = wrap(x - o, X) * 2 + c
            tcopy(l, slot, partner, 0).wait_recv()
            go(None, lambda o=o, slot=slot: tcopy(l, slot, partner, X - 1 + o))

    def tok_fin(l):
        for o in range(X):
            tcopy(l, wrap(x - o, X) * 2 + 1 - c, partner, 0).wait_recv()

    NC = C // LANES

    def project(l):
        def mb(i, _):
            r = pl.ds(pl.multiple_of(i * RT, RT), RT)
            a = TOK[l, r, :]
            lin = dot(a, WV[l])
            gate = dot(a, WG[l])
            glu = (lin * jax.nn.sigmoid(gate)).astype(BF16).astype(F32)
            for n in range(NC):
                GLF[n, pl.ds(pl.multiple_of(HALO + i * RT, 8), RT), :] = glu[:, n * LANES:(n + 1) * LANES]
            return 0
        lax.fori_loop(0, M // RT, mb, 0)
        for n in range(NC):
            HB[l, 0, :, n * LANES:(n + 1) * LANES] = GLF[n, M:M + HALO, :].astype(BF16)
        go(s + 1 < Z * Y, lambda: hcopy(l))

    def hcopy(l):
        return pltpu.make_async_remote_copy(
            src_ref=HB.at[l, 0], dst_ref=HB.at[l, 1], send_sem=h_ss.at[l], recv_sem=h_rs.at[l],
            device_id=nxt, device_id_type=MESH)

    def halo_fin(l):
        @pl.when(s >= 1)
        def _():
            hcopy(l).wait_recv()
            for n in range(NC):
                GLF[n, 0:HALO, :] = HB[l, 1, :, n * LANES:(n + 1) * LANES].astype(F32)

        @pl.when(s == 0)
        def _():
            for n in range(NC):
                GLF[n, 0:HALO, :] = jnp.zeros((HALO, LANES), F32)

    CT = 64

    def conv_tile(l, i):
        first = HALO - (taps - 1)
        s1 = jnp.zeros((CT, LANES), F32)
        s2 = jnp.zeros((CT, LANES), F32)
        base = pl.multiple_of(i * CT, CT)
        for n in range(NC):
            lanes = slice(n * LANES, (n + 1) * LANES)
            acc = jnp.zeros((CT, LANES), F32) + cb_ref[l:l + 1, lanes]
            for tap in range(taps):
                acc = acc + cw_ref[l, tap:tap + 1, lanes] * GLF[n, pl.ds(base + first + tap, CT), :]
            MIX[pl.ds(base, CT), lanes] = acc
            s1 = s1 + acc
            s2 = s2 + acc * acc
        S1[pl.ds(base, CT), :] = s1
        S2[pl.ds(base, CT), :] = s2

    def conv(l, lo, hi):
        def cbody(i, _):
            conv_tile(l, i)
            return 0
        lax.fori_loop(lo, hi, cbody, 0)

    def scopy(l, o):
        return pltpu.make_async_remote_copy(
            src_ref=ST.at[l, 0], dst_ref=ST.at[l, o], send_sem=s_ss.at[l, o - 1], recv_sem=s_rs.at[l, o - 1],
            device_id=(s, wrap(t + o, NT)), device_id_type=MESH)

    def stats_send(l):
        for i in range(M // RT):
            r = slice(i * RT, (i + 1) * RT)
            a = jnp.sum(jnp.transpose(S1[r, :]), axis=0, keepdims=True)
            b = jnp.sum(jnp.transpose(S2[r, :]), axis=0, keepdims=True)
            ST[l, 0, 0:1, r] = a
            ST[l, 0, 1:2, r] = b
        ST[l, 0, 2:8, :] = jnp.zeros((6, M), F32)
        for o in range(1, NT):
            go(None, lambda o=o: scopy(l, o))

    def activate(l):
        for o in range(1, NT):
            scopy(l, o).wait_recv()
        for i in range(M // RT):
            r = slice(i * RT, (i + 1) * RT)
            tot = ST[l, 0, :, r]
            for o in range(1, NT):
                tot = tot + ST[l, o, :, r]
            tot = tot / (C * NT)
            mean = tot[0:1, :]
            var = tot[1:2, :] - mean * mean
            inv = lax.rsqrt(var + EPS)
            mb = jnp.transpose(jnp.broadcast_to(mean, (LANES, RT)))
            ib = jnp.transpose(jnp.broadcast_to(inv, (LANES, RT)))
            S1[r, :] = mb
            S2[r, :] = ib

        def ab(i, _):
            r = pl.ds(pl.multiple_of(i * CT, CT), CT)
            mb, ib = S1[r, :], S2[r, :]
            for n in range(NC):
                lanes = slice(n * LANES, (n + 1) * LANES)
                v = (MIX[r, lanes] - mb) * ib * cg_ref[l:l + 1, lanes] + cs_ref[l:l + 1, lanes]
                ACT[r, lanes] = (v / (1.0 + jnp.exp(-v))).astype(BF16)
            return 0
        lax.fori_loop(0, M // CT, ab, 0)

    def dcopy(l, src):
        return pltpu.make_async_remote_copy(
            src_ref=PT.at[l, src, pl.ds(X, X)], dst_ref=PI.at[l, src],
            send_sem=d_ss.at[l, src], recv_sem=d_rs.at[l, src], device_id=partner, device_id_type=MESH)

    def xcopy(l, src, o):
        return pltpu.make_async_remote_copy(
            src_ref=PX.at[l, src, o - 1], dst_ref=RX.at[l, src, o - 1],
            send_sem=x_ss.at[l, src, o - 1], recv_sem=x_rs.at[l, src, o - 1],
            device_id=tdev(wrap(x + o, X), c), device_id_type=MESH)

    def chunk(l, src):
        def qb(q, _):
            off, other = lax.rem(q, X), q // X
            cc = jnp.where(other == 0, c, 1 - c)
            td = lax.rem(x + off, X) * 2 + cc
            a = ACT[pl.ds(pl.multiple_of(td * own_rows, own_rows), own_rows), :]
            PT[l, src, q] = dot(a, WO[l, src]).astype(BF16)
            return 0
        lax.fori_loop(0, 2 * X, qb, 0)
        go(None, lambda: dcopy(l, src))

    def chunk_x(l, src):
        dcopy(l, src).wait_recv()
        for o in range(1, X):
            PX[l, src, o - 1] = (PT[l, src, o].astype(F32) + PI[l, src, o].astype(F32)).astype(BF16)
            go(None, lambda o=o: xcopy(l, src, o))

    def finish(l):
        last = l == L - 1
        for src in range(Z * Y):
            upd = PT[l, src, 0].astype(F32) + PI[l, src, 0].astype(F32)
            for o in range(1, X):
                xcopy(l, src, o).wait_recv()
                upd = upd + RX[l, src, o - 1].astype(F32)
            cols = slice(src * wcols, (src + 1) * wcols)
            old = (h_ref if l == 0 else HS)[:, cols].astype(F32)
            (o_ref if last else HS)[:, cols] = (old + upd).astype(BF16)

    state = {"prev": None}

    def do_chunk(l, j, yo):
        src = zorder(j) * Y + wrap(y + yo, Y)
        chunk(l, src)
        if state["prev"] is not None:
            chunk_x(*state["prev"])
        state["prev"] = (l, src)

    def flush_chunk():
        chunk_x(*state["prev"])
        state["prev"] = None

    send_own(0)
    send_own(1)
    norm_send(0)
    for l in range(L):
        v, g, w = 3 * l, 3 * l + 1, 3 * l + 2
        more = l + 1 < L
        if l == 0:
            ev_d(v, 1)
            for k in range(2, Z):
                ev_d(v, k)
            send_own(w)
            tok_relay(l)
            ev_d(g, 1)
            for k in range(2, Z):
                ev_d(g, k)
            if scheme_a[w]:
                ev_p(w)
            if more:
                send_own(v + 3)
            ev_d(w, 1)
        fin(v)
        fin(g)
        tok_fin(l)
        project(l)
        if l > 0:
            for k in range(1, Z - 1):
                ev_d(w, k)
        conv(l, 1, M // CT // 2)
        if l == 0 and Z > 2:
            ev_d(w, 2)
        conv(l, M // CT // 2, M // CT)
        halo_fin(l)
        conv(l, 0, 1)
        stats_send(l)
        if more:
            for k in range(3, Z):
                ev_d(w, k)
            send_own(g + 3)
            ev_d(v + 3, 1)
        activate(l)
        if more:
            do_chunk(l, 0, 0)
            ev_d(v + 3, 2)
            send_own(w + 3)
        else:
            do_chunk(l, 0, 0)
            ev_d(w, Z - 1)
        for j in range(1, Z):
            do_chunk(l, j, 0)
        if more:
            for k in range(3, Z):
                ev_d(v + 3, k)
        for j in range(Z):
            for yo in range(1, Y):
                if not scheme_a[w]:
                    wait_w(w, zorder(j) * Y + wrap(y + yo, Y))
                do_chunk(l, j, yo)
        flush_chunk()
        if more:
            ev_d(g + 3, 1)
        finish(l)
        if more:
            norm_send(l + 1)
            for k in range(2, Z):
                ev_d(g + 3, k)
            tok_relay(l + 1)
    drain()


def solution(mesh):
    sp, tp = mesh.shape["sp"], mesh.shape["tp"]
    Y = 1
    while (2 * Y) * (2 * Y) <= sp:
        Y *= 2
    Z, X = sp // Y, tp // 2

    def body(*args):
        hidden, norm_gain, w_value, w_gate, conv_weight, conv_bias, chan_gain, chan_shift, w_out = args
        own_rows, D = hidden.shape
        L, rows, C = w_value.shape
        wcols = w_out.shape[2]
        M = own_rows * tp
        U = 3 * L
        vm = pltpu.VMEM
        dma = pltpu.SemaphoreType.DMA
        nx = max(X - 1, 1)
        return pl.pallas_call(
            functools.partial(kernel, Z, Y, X),
            out_shape=jax.ShapeDtypeStruct((own_rows, D), BF16),
            in_specs=[pl.BlockSpec(memory_space=pltpu.VMEM)] * 9,
            out_specs=pl.BlockSpec(memory_space=pltpu.VMEM),
            scratch_shapes=[
                vm((L, sp * rows, C), BF16), vm((L, sp * rows, C), BF16), vm((L, sp, C, wcols), BF16),
                vm((L, M, D), BF16),
                vm((L, sp, 2 * X, own_rows, wcols), BF16), vm((L, sp, X, own_rows, wcols), BF16),
                vm((L, sp, nx, own_rows, wcols), BF16), vm((L, sp, nx, own_rows, wcols), BF16),
                vm((C // LANES, HALO + M, LANES), F32), vm((L, 2, HALO, C), BF16),
                vm((M, C), F32), vm((M, LANES), F32), vm((M, LANES), F32),
                vm((L, tp, 8, M), F32), vm((M, C), BF16), vm((own_rows, D), BF16),
                dma((U, sp)), dma((U, sp)), dma((U, Y)), dma((U, Z, max(Y - 1, 1))),
                dma((L, 2 * X)), dma((L, tp)), dma((L,)), dma((L,)), dma((L, tp - 1)), dma((L, tp - 1)),
                dma((L, sp)), dma((L, sp)), dma((L, sp, nx)), dma((L, sp, nx)),
            ],
            compiler_params=pltpu.CompilerParams(
                collective_id=0, has_side_effects=True, vmem_limit_bytes=65000 * 1024),
        )(*args)

    placed = (
        P(("sp", "tp"), None), P(), P(None, "sp", "tp"), P(None, "sp", "tp"), P(None, None, "tp"),
        P(None, "tp"), P(None, "tp"), P(None, "tp"), P(None, "tp", "sp"),
    )
    return jax.shard_map(
        body, mesh=mesh, in_specs=placed, out_specs=P(("sp", "tp"), None), check_vma=False)
```

time: 467 us -> 175 us (0.37)
  waiting for transfers between devices: 382 us -> 0 us
  Pallas kernels: 0 us -> 171 us
  matrix products: 28.3 us -> 0 us
  other arithmetic: 20.8 us -> 0 us
  between operations: 13.8 us -> 0.01 us
  blocking collectives: 12.3 us -> 0 us
  starting transfers between devices: 5.48 us -> 0 us
    all_gather x8 -> x0, waiting for transfers between devices: 305 us -> none  [the longest x2 95.9 us: body(): lax.all_gather(w_gate[layer], 'sp', axis=0, tiled=True)]
    pallas_call x0 -> x1, Pallas kernels: none -> 171 us  [body(): pl.pallas_call(functools.partial(kernel, Z, Y, X), out_shape=jax.ShapeDty...]
    reduce_scatter x2 -> x0, waiting for transfers between devices: 71.8 us -> none  [body(): lax.psum_scatter(take_rows(jnp.int32(0), own_rows * lax.axis_size('tp'))....]
    dot_general x6 -> x0, matrix products: 28.3 us -> none  [the longest x2 10.7 us: project(): return jnp.dot(act, piece, preferred_element_type=jnp.float32)]
    reduce_sum x4 -> x0, other arithmetic: 15.6 us -> none  [the longest x2 13.8 us: body(): jnp.sum(mixed, axis=1)]
    psum x2 -> x0, blocking collectives: 12.3 us -> none  [body(): lax.psum((jnp.sum(mixed, axis=1), jnp.sum(mixed * mixed, axis=1)), 'tp')]
    convert_element_type x5 -> x0, other arithmetic: 5.23 us -> none  [the longest x1 2.4 us: body(): state = (xf + update).astype(jnp.bfloat16)]
    ppermute x2 -> x0, starting transfers between devices: 5.12 us -> none  [shifted(): return lax.ppermute(shard, axis, pairs)]
  transfers between devices with their start and end apart: 12 -> 0, of which waited for: 12 -> 0; matrix products, arithmetic and copies ran while one was open for 8% -> 0% of each run, Pallas kernels for 0% -> 0%
where the time goes in v1:
time: 175 us
  Pallas kernels  171 us (98%)
  local copies, waits for them, and re-layouts  3.67 us (2%)
    pallas_call x1, Pallas kernels, body(): pl.pallas_call(functools.partial(kernel, Z, Y, X), out_shape=jax.ShapeDty...  171 us
    unnamed x2, local copies, waits for them, and re-layouts  3.67 us

profile of v1, /device:TPU:0, one launch (start us, length us, event | category | flops | bytes accessed | tf_op | source)
XLA Modules:
  0.0 174.9 jit_solution(5620678979165797164)
XLA Ops:
  0.0 1.6 copy.10.cw_ref
  1.6 171.2 %shard_map.91 = bf16[192,2048]{1,0:T(8,128)(2,1)} custom-call(bf16[192,2048]{1,0:T(8,128)(2,1)} %h_ref.1, f32[2,2048]{1,0:T(2,128)} %gain_ref.1, bf16[2,256,512]{2,1,0:T(8,128)(2,1)} %wv_ref.1, bf16[2,256,512]{2,1,0:T(8,128)(2,1)} %wg_ref.1, f32[2,31,512]{2,1,0:T(8,128)} %copy.10.cw_ref, f32[2,512]{1,0:T(2,128)} %cb_ref.1, f32[2,512]{1,0:T(2,128)} %cg_ref.1, ...), custom_call_target="tpu_custom_call" | custom-call | tf_op jit(solution)/shard_map/pallas_call | solution.py:454
  172.8 2.1 %copy.12 = bf16[192,2048]{1,0:T(8,128)(2,1)} copy(bf16[192,2048]{1,0:T(8,128)(2,1)} %shard_map.91) | data formatting | bytes 1572864

commit v2 on v1

--- a/solution.py
+++ b/solution.py
@@ -37,7 +37,7 @@
     x, c = t // 2, lax.rem(t, 2)
     units = [(l, k) for l in range(L) for k in range(3)]
     U = len(units)
-    scheme_a = [u == 2 for u in range(U)]
+    scheme_a = [u == 3 for u in range(U)]
 
     def wrap(v, n):
         return lax.rem(v + n, n)
@@ -365,6 +365,10 @@
         chunk_x(*state["prev"])
         state["prev"] = None
 
+    def ev_rest(u, k0):
+        for k in range(k0, Z):
+            ev_d(u, k)
+
     send_own(0)
     send_own(1)
     norm_send(0)
@@ -373,64 +377,55 @@
         more = l + 1 < L
         if l == 0:
             ev_d(v, 1)
-            for k in range(2, Z):
-                ev_d(v, k)
+            ev_d(v, 2)
             send_own(w)
+            ev_rest(v, 3)
             tok_relay(l)
             ev_d(g, 1)
-            for k in range(2, Z):
-                ev_d(g, k)
-            if scheme_a[w]:
-                ev_p(w)
+            ev_d(g, 2)
             if more:
                 send_own(v + 3)
+            ev_rest(g, 3)
             ev_d(w, 1)
         fin(v)
         fin(g)
         tok_fin(l)
         project(l)
-        if l > 0:
-            for k in range(1, Z - 1):
-                ev_d(w, k)
+        if l == 0:
+            ev_d(w, 2)
+            if more:
+                send_own(g + 3)
+                if scheme_a[v + 3]:
+                    ev_p(v + 3)
         conv(l, 1, M // CT // 2)
-        if l == 0 and Z > 2:
-            ev_d(w, 2)
+        if l == 0:
+            ev_rest(w, 3)
         conv(l, M // CT // 2, M // CT)
         halo_fin(l)
         conv(l, 0, 1)
         stats_send(l)
         if more:
-            for k in range(3, Z):
-                ev_d(w, k)
-            send_own(g + 3)
             ev_d(v + 3, 1)
         activate(l)
-        if more:
-            do_chunk(l, 0, 0)
-            ev_d(v + 3, 2)
-            send_own(w + 3)
-        else:
-            do_chunk(l, 0, 0)
-            ev_d(w, Z - 1)
-        for j in range(1, Z):
-            do_chunk(l, j, 0)
-        if more:
-            for k in range(3, Z):
-                ev_d(v + 3, k)
-        for j in range(Z):
-            for yo in range(1, Y):
-                if not scheme_a[w]:
+        for yo in range(Y):
+            for j in range(Z):
+                if yo > 0 and not scheme_a[w]:
                     wait_w(w, zorder(j) * Y + wrap(y + yo, Y))
                 do_chunk(l, j, yo)
         flush_chunk()
         if more:
+            ev_d(v + 3, 2)
+            send_own(w + 3)
+            ev_rest(v + 3, 3)
             ev_d(g + 3, 1)
         finish(l)
         if more:
+            ev_d(g + 3, 2)
             norm_send(l + 1)
-            for k in range(2, Z):
-                ev_d(g + 3, k)
+            ev_rest(g + 3, 3)
+            ev_d(w + 3, 1)
             tok_relay(l + 1)
+            ev_rest(w + 3, 2)
     drain()
 
 

time: 175 us -> 177 us (1.011)
  no operation moved by 1% of the time
where the time goes in v2:
time: 177 us; the launch traced here: 176 us
  Pallas kernels  172 us (97%)
  local copies, waits for them, and re-layouts  3.67 us (2%)
    pallas_call x1, Pallas kernels, body(): pl.pallas_call(functools.partial(kernel, Z, Y, X), out_shape=jax.ShapeDty...  172 us
    unnamed x2, local copies, waits for them, and re-layouts  3.67 us

profile of v2, /device:TPU:0, one launch (start us, length us, event | category | flops | bytes accessed | tf_op | source)
XLA Modules:
  0.0 175.8 jit_solution(6501778447175964202)
XLA Ops:
  0.0 1.6 copy.10.cw_ref
  1.6 172.1 %shard_map.91 = bf16[192,2048]{1,0:T(8,128)(2,1)} custom-call(bf16[192,2048]{1,0:T(8,128)(2,1)} %h_ref.1, f32[2,2048]{1,0:T(2,128)} %gain_ref.1, bf16[2,256,512]{2,1,0:T(8,128)(2,1)} %wv_ref.1, bf16[2,256,512]{2,1,0:T(8,128)(2,1)} %wg_ref.1, f32[2,31,512]{2,1,0:T(8,128)} %copy.10.cw_ref, f32[2,512]{1,0:T(2,128)} %cb_ref.1, f32[2,512]{1,0:T(2,128)} %cg_ref.1, ...), custom_call_target="tpu_custom_call" | custom-call | tf_op jit(solution)/shard_map/pallas_call | solution.py:449
  173.7 2.1 %copy.12 = bf16[192,2048]{1,0:T(8,128)(2,1)} copy(bf16[192,2048]{1,0:T(8,128)(2,1)} %shard_map.91) | data formatting | bytes 1572864
